TPU v7x, 256 devices: a whole 4x4x8 slice. The times are simulated.
256 devices in a mesh: sp: 32 (over z, x), tp: 8 (over y, core).
Axes of the slice: x: 4, y: 4, z: 8, core: 2. Of those that a mesh axis runs over, the one named last changes fastest.
Arguments:
- tokens: bfloat16 [2, 6144, 4096], P(None, 'sp', 'tp'), may hold values from -12 to 12
- query_weight: bfloat16 [4096, 2048], P(None, 'tp'), may hold values from -0.09375 to 0.09375
- key_weight: bfloat16 [4096, 2048], P(None, 'tp'), may hold values from -0.09375 to 0.09375
- value_weight: bfloat16 [4096, 2048], P(None, 'tp'), may hold values from -0.09375 to 0.09375
- gate_weight: bfloat16 [4096, 2048], P(None, 'tp'), may hold values from -0.09375 to 0.09375
- beta_weight: bfloat16 [4096, 16], P(None, 'tp'), may hold values from -0.09375 to 0.09375
- decay_weight: bfloat16 [4096, 16], P(None, 'tp'), may hold values from -0.09375 to 0.09375
- beta_bias: float32 [16], P('tp'), may hold values from -6 to -3
- rate_log: float32 [16], P('tp'), may hold values from -12 to -2.5
- out_gain: float32 [128], replicated, may hold values from 0.1 to 1.9
- new_query: bfloat16 [2, 16, 128], P(None, 'tp'), may hold values from -6 to 6
- new_key: bfloat16 [2, 16, 128], P(None, 'tp'), may hold values from -6 to 6
- new_value: bfloat16 [2, 16, 128], P(None, 'tp'), may hold values from -6 to 6
- new_beta: float32 [2, 16], P(None, 'tp'), may hold values from 0.1 to 0.9
- new_decay: float32 [2, 16], P(None, 'tp'), may hold values from 0.3 to 1
Outputs:
- mixed_out: bfloat16 [2, 6144, 2048], P(None, 'sp', 'tp')
- cache: bfloat16 [2, 16, 128, 128], P(None, 'tp', 'sp')
- first_out: float32 [2, 2048], P(None, 'tp')
All inputs are finite; a program needn't handle non-finite values.
Results may differ from a plain program's by a relative error of at most 0.0073.
Values may be sent and summed in bfloat16 or wider, within the bound.
No kernel may reach another device: no remote copies, remote signals or barrier semaphores. Data moves between devices by JAX's collectives and lax.ppermute only.
A program may use at most 64 MiB of HBM per device.

v0:
```python
import jax
import jax.numpy as jnp
from jax import lax
from jax.sharding import Mesh
from jax.sharding import PartitionSpec as P

BLOCK = 64
SP = ("sp_0", "sp_1")
unit_floor = 1.0
norm_floor = 0.001
highest = lax.Precision.HIGHEST


def neutral_like(value, identity):
    return jax.tree.map(
        lambda a, e: jnp.broadcast_to(jnp.asarray(e, a.dtype), a.shape), value, identity
    )


def carried_in(value, axes, combine, identity):
    before = start = neutral_like(value, identity)
    subtotal = value
    for axis in reversed(axes):
        length, index = (lax.axis_size(axis), lax.axis_index(axis))
        pieces = jax.tree.map(lambda part: lax.all_gather(part, axis), subtotal)
        inside, subtotal = (start, start)
        for k in range(length):
            passed = k < index
            subtotal = combine(subtotal, jax.tree.map(lambda part: part[k], pieces))
            inside = jax.tree.map(lambda new, old: jnp.where(passed, new, old), subtotal, inside)
        before = combine(inside, before)
    return before


def split_up(value, dim, length):
    before, after = (value.shape[:dim], value.shape[dim + 1 :])
    return jnp.moveaxis(value.reshape(*before, length, -1, *after), dim, 0)


def summed_on_arrival(value, axis, dim):
    parts = split_up(value, dim, lax.axis_size(axis))
    arrived = lax.all_to_all(parts, axis, split_axis=0, concat_axis=0, tiled=True)
    return arrived.astype(jnp.float32).sum(axis=0)


def copy_for_each(value, axis):
    length = lax.axis_size(axis)
    return lax.all_to_all(
        jnp.broadcast_to(value[None], (length, *value.shape)), axis, 0, 0, tiled=True
    )


def over_copies(value, axis):
    everything = copy_for_each(value, axis)
    return jnp.sum(everything, axis=0)


def in_one(arrays, axis):
    ravelled, at, gathered = (jnp.concatenate([a.reshape(-1) for a in arrays]), 0, [])
    subtotal = over_copies(ravelled, axis)
    for a in arrays:
        gathered.append(subtotal[at : at + a.size].reshape(a.shape))
        at += a.size
    return tuple(gathered)


def matmul(form, left, right):
    return jnp.einsum(form, left, right, precision=highest)


def unit_rows(values):
    return values * lax.rsqrt(jnp.sum(values * values, axis=-1, keepdims=True) + unit_floor)


def head_norm(values, out_gain):
    return (
        values
        * lax.rsqrt(jnp.mean(values * values, axis=-1, keepdims=True) + norm_floor)
        * out_gain
    )


def stored(values):
    return lax.optimization_barrier(values.astype(jnp.bfloat16)).astype(jnp.float32)


def unit_lower_inverse(lower_part):
    extent = lower_part.shape[-1]
    nilpotent = -lower_part
    inverse = jnp.eye(extent, dtype=jnp.float32) + nilpotent
    for _ in range(extent.bit_length() - 2):
        nilpotent = matmul("...ij,...jk->...ik", nilpotent, nilpotent)
        inverse = inverse + matmul("...ij,...jk->...ik", nilpotent, inverse)
    return inverse


def prepare(
    query_rows,
    key_rows,
    value_rows,
    beta_in,
    decay_in,
    beta_bias,
    rate_log,
    seq_count,
    length,
    head_count,
):
    extent = query_rows.shape[-1] // head_count
    blocks = length // BLOCK

    def by_head(values):
        shaped = values.reshape(seq_count, blocks, BLOCK, head_count, extent)
        return shaped.transpose(0, 3, 1, 2, 4).reshape(
            seq_count * head_count, blocks, BLOCK, extent
        )

    def by_scalar(values):
        shaped = values.reshape(seq_count, blocks, BLOCK, head_count)
        return shaped.transpose(0, 3, 1, 2).reshape(seq_count * head_count, blocks, BLOCK)

    queries = unit_rows(by_head(query_rows))
    key_unit = unit_rows(by_head(key_rows))
    values = by_head(value_rows)
    strength = by_scalar(jax.nn.sigmoid(beta_in + beta_bias))
    decays = by_scalar(-jnp.exp(rate_log) * jax.nn.softplus(decay_in))
    return (queries, key_unit, values, strength, decays)


def block_terms(queries, key_unit, values, strength, decays):
    extent = decays.shape[-1]
    cumulative = jnp.cumsum(decays, axis=-1)
    causal = jnp.tril(jnp.ones((extent, extent), bool))
    strict = jnp.tril(jnp.ones((extent, extent), bool), -1)
    spread = cumulative[..., :, None] - cumulative[..., None, :]
    weights = jnp.where(causal, jnp.exp(jnp.where(causal, spread, 0.0)), 0.0)
    key_beta = key_unit * strength[..., None]
    lower_part = jnp.where(strict, matmul("...td,...sd->...ts", key_beta, key_unit) * weights, 0.0)
    inverse = unit_lower_inverse(lower_part)
    update = matmul("...ts,...se->...te", inverse, values * strength[..., None])
    carry_w = matmul("...ts,...sd->...td", inverse, key_beta * jnp.exp(cumulative)[..., None])
    scores = matmul("...td,...sd->...ts", queries, key_unit) * weights
    query_decay = queries * jnp.exp(cumulative)[..., None]
    last_log = cumulative[..., -1]
    key_decay = key_unit * jnp.exp(last_log[..., None] - cumulative)[..., None]
    return (update, carry_w, query_decay, scores, key_decay, last_log)


def finish_read(recall, retrieve, query_unit, key_unit, new_value, new_beta, new_decay, out_gain):
    seq_count, head_count, extent = recall.shape
    intersect = jnp.sum(key_unit * query_unit, axis=-1)
    fresh_values = new_value.astype(jnp.float32) - new_decay[..., None] * retrieve
    read_heads = new_decay[..., None] * recall + (new_beta * intersect)[..., None] * fresh_values
    return head_norm(read_heads, out_gain).reshape(seq_count, head_count * extent)


def project_rows(shard_rows, weights):
    row_count = shard_rows.shape[-1]
    flat_rows = shard_rows.reshape(-1, row_count)
    return tuple(
        (jnp.dot(flat_rows, weight, preferred_element_type=jnp.float32) for weight in weights)
    )


def shards(
    tokens,
    query_weight,
    key_weight,
    value_weight,
    gate_weight,
    beta_weight,
    decay_weight,
    beta_bias,
    rate_log,
    out_gain,
    new_query,
    new_key,
    new_value,
    new_beta,
    new_decay,
):
    seq_count, span_len, _ = tokens.shape
    head_count = rate_log.shape[0]
    weights = (query_weight, key_weight, value_weight, gate_weight, beta_weight, decay_weight)
    totals = project_rows(lax.all_gather(tokens, "tp", axis=2, tiled=True), weights)
    query_rows = stored(totals[0])
    key_rows = stored(totals[1])
    value_rows = stored(totals[2])
    gate_rows = stored(totals[3])
    prepared = prepare(
        query_rows,
        key_rows,
        value_rows,
        totals[4],
        totals[5],
        beta_bias,
        rate_log,
        seq_count,
        span_len,
        head_count,
    )
    block_data = block_terms(*prepared)
    batch_size = block_data[0].shape[0]
    extent = block_data[0].shape[-1]
    identity = jnp.broadcast_to(jnp.eye(extent, dtype=jnp.float32), (batch_size, extent, extent))

    def advance(carried, inputs):
        state_now, reach_map = carried
        u_block, w_block, qg_block, score_block, kd_block, gl_block = inputs
        fresh_values = u_block - matmul("btd,bde->bte", w_block, state_now)
        block_out = matmul("btd,bde->bte", qg_block, state_now) + matmul(
            "bts,bse->bte", score_block, fresh_values
        )
        reach_rows = qg_block - matmul("bts,bsd->btd", score_block, w_block)
        factor = jnp.exp(gl_block)[:, None, None]
        transit = factor * identity - matmul("bsd,bse->bde", kd_block, w_block)
        state_next = state_now * factor + matmul("bsd,bse->bde", kd_block, fresh_values)
        map_next = matmul("bde,bef->bdf", transit, reach_map)
        return ((state_next, map_next), (block_out, matmul("btd,bde->bte", reach_rows, reach_map)))

    inputs = tuple((jnp.moveaxis(member, 1, 0) for member in block_data))
    start_state = jnp.zeros((batch_size, extent, extent), jnp.float32)
    (local_state, local_map), (local_out, reach_all) = lax.scan(
        advance, (start_state, identity), inputs
    )

    def compose(earlier, later):
        return (
            matmul("bde,bef->bdf", later[0], earlier[0]),
            matmul("bde,bef->bdf", later[0], earlier[1]) + later[1],
        )

    prefix = carried_in(
        (local_map, local_state), SP, compose, (identity, jnp.zeros_like(local_state))
    )
    incoming = prefix[1]
    block_total = local_out + matmul("nbtd,bde->nbte", reach_all, incoming)
    blocks = span_len // BLOCK
    heads_out = block_total.reshape(blocks, seq_count, head_count, BLOCK, extent).transpose(
        1, 0, 3, 2, 4
    )
    heads_out = heads_out.reshape(seq_count, span_len, head_count, extent)
    gate_values = gate_rows.reshape(seq_count, span_len, head_count, extent)
    mixed_out = (head_norm(heads_out, out_gain) * jax.nn.silu(gate_values)).astype(jnp.bfloat16)
    mixed_out = mixed_out.reshape(seq_count, span_len, head_count * extent)
    final_state = matmul("bde,bef->bdf", local_map, incoming) + local_state
    final_cast = final_state.reshape(seq_count, head_count, extent, extent).astype(jnp.bfloat16)
    row_count = extent // lax.axis_size(SP)
    row_start = lax.axis_index(SP) * row_count
    query_unit = unit_rows(new_query.astype(jnp.float32))
    key_unit = unit_rows(new_key.astype(jnp.float32))
    is_last = lax.axis_index(SP) == lax.axis_size(SP) - 1
    own_term = jnp.where(is_last, final_cast.astype(jnp.float32), 0.0)
    cache_rows = summed_on_arrival(own_term.astype(jnp.bfloat16), SP, 2).astype(jnp.bfloat16)
    memory = lax.optimization_barrier(cache_rows).astype(jnp.float32)
    query_part = lax.dynamic_slice_in_dim(query_unit, row_start, row_count, 2)
    key_part = lax.dynamic_slice_in_dim(key_unit, row_start, row_count, 2)
    recall, retrieve = in_one(
        (matmul("shde,shd->she", memory, query_part), matmul("shde,shd->she", memory, key_part)), SP
    )
    first_out = finish_read(
        recall, retrieve, query_unit, key_unit, new_value, new_beta, new_decay, out_gain
    )
    return (mixed_out, cache_rows, first_out)


def solution(mesh):
    torus = Mesh(mesh.devices.reshape(8, 4, mesh.shape["tp"]), ("sp_0", "sp_1", "tp"))
    in_specs = (
        P(None, SP, "tp"),
        P(None, "tp"),
        P(None, "tp"),
        P(None, "tp"),
        P(None, "tp"),
        P(None, "tp"),
        P(None, "tp"),
        P("tp"),
        P("tp"),
        P(),
        P(None, "tp", None),
        P(None, "tp", None),
        P(None, "tp", None),
        P(None, "tp"),
        P(None, "tp"),
    )
    out_specs = (P(None, SP, "tp"), P(None, "tp", SP, None), P(None, "tp"))
    return jax.shard_map(
        shards, mesh=torus, in_specs=in_specs, out_specs=out_specs, check_vma=False
    )
```

profile of v0, /device:TPU:8, one launch (start us, length us, event | category | flops | bytes accessed | tf_op | source)
XLA Modules:
  0.0 295.3 jit_solution(3390538268324986770)
XLA Ops:
  9.4 32.6 %all-gather.10.cloned.1.call-done = bf16[2,192,4096]{2,1,0:T(8,128)(2,1)} async-done(((bf16[2,192,512]{2,1,0:T(8,128)(2,1)}), bf16[2,192,4096]{2,1,0:T(8,128)(2,1)}) %all-gather.10.cloned.1.call-update) | async-done | bytes 3145744 | tf_op jit(solution)/shard_map/all_gather | solution.py:185
  42.0 2.8 fusion.91
  45.0 1.0 reduce_window_sum.11
  46.8 2.9 convolution_convert_fusion.1
  50.4 0.8 copy.189
  51.3 2.8 fusion.50
  54.3 3.5 %convolution_convert_fusion.3 = bf16[384,256]{1,0:T(8,128)(2,1)S(1)} fusion(bf16[384,4096]{1,0:T(8,128)(2,1)} %bitcast.236, bf16[4096,256]{1,0:T(8,128)(2,1)} %param.19), kind=kOutput, calls=%fused_computation.61 | convolution fusion | flops 805404672 | bytes 5439488 | tf_op jit(solution)/shard_map/dot_general | solution.py:161
  58.5 0.8 copy.178
  59.4 3.6 %convolution_convert_fusion.2 = bf16[384,256]{1,0:T(8,128)(2,1)S(1)} fusion(bf16[384,4096]{1,0:T(8,128)(2,1)} %bitcast.237, bf16[4096,256]{1,0:T(8,128)(2,1)} %param.20), kind=kOutput, calls=%fused_computation.60 | convolution fusion | flops 805404672 | bytes 5439488 | tf_op jit(solution)/shard_map/dot_general | solution.py:161
  63.3 1.5 multiply_bitcast_fusion
  64.8 0.9 multiply_bitcast_fusion.1
  65.7 0.8 fusion.41
  71.8 1.3 convolution_bitcast_fusion.4
  73.1 0.7 convolution_bitcast_fusion.3
  73.8 1.5 fusion.39
  75.3 29.5 %while.17 = (s32[]{:T(128)}, f32[4,128,128]{2,1,0:T(8,128)S(1)}, f32[4,128,128]{2,1,0:T(8,128)S(1)}, f32[3,4,64,128]{3,2,0,1:T(8,128)}, f32[3,4,64,128]{3,2,0,1:...) while((s32[]{:T(128)}, f32[4,128,128]{2,1,0:T(8,128)S(1)}, ...), condition=%wide.region_4.5_spmd.clone, body=%wide.region_3.4_spmd.clone.sunk | while | flops 403210240 | bytes 5445847 | solution.py:223
  75.3 1.3 convolution_subtract_fusion.6
  76.6 1.2 fusion.226
  77.8 1.0 fusion.227
  79.5 1.5 convolution_add_fusion.23
  81.0 1.2 convolution_subtract_fusion.8
  82.2 1.0 fusion.228
  83.2 1.5 convolution_subtract_fusion.7
  85.2 1.3 convolution_subtract_fusion.6
  86.4 1.2 fusion.226
  87.6 1.0 fusion.227
  89.3 1.5 convolution_add_fusion.23
  90.8 1.2 convolution_subtract_fusion.8
  92.0 1.0 fusion.228
  93.1 1.5 convolution_subtract_fusion.7
  95.0 1.3 convolution_subtract_fusion.6
  96.3 1.2 fusion.226
  97.5 1.0 fusion.227
  99.2 1.5 convolution_add_fusion.23
  100.7 1.2 convolution_subtract_fusion.8
  101.9 1.0 fusion.228
  102.9 1.5 convolution_subtract_fusion.7
  104.9 0.7 copy-done.4
  106.4 26.9 %all-gather.12.cloned.1.call-done = f32[16,128,128]{2,1,0:T(8,128)} async-done(((f32[4,128,128]{2,1,0:T(8,128)}), f32[16,128,128]{2,1,0:T(8,128)}) %all-gather.12.cloned.1.call-update) | async-done | bytes 1048592 | tf_op jit(solution)/shard_map/all_gather | solution.py:25
  133.3 1.4 fusion.76
  134.7 0.7 copy-done.17
  135.4 1.3 fusion.107
  136.8 0.7 copy-done.7
  137.9 0.7 copy-done.9
  138.6 1.1 fusion.109
  139.8 22.4 %all-gather.16.cloned.1.call-done = f32[16,128,128]{2,1,0:T(8,128)} async-done(((f32[4,128,128]{2,1,0:T(8,128)}), f32[16,128,128]{2,1,0:T(8,128)}) %all-gather.16.cloned.1.call-update) | async-done | bytes 1048592 | tf_op jit(solution)/shard_map/all_gather | solution.py:25
  162.2 1.4 convolution_add_fusion.19
  163.6 1.4 convolution_add_fusion.18
  165.0 0.7 copy-done.13
  166.8 1.1 convolution_add_fusion.16
  168.5 4.3 %convolution_convert_fusion = bf16[384,256]{1,0:T(8,128)(2,1)} fusion(bf16[384,4096]{1,0:T(8,128)(2,1)} %bitcast.238, bf16[4096,256]{1,0:T(8,128)(2,1)} %param.21), kind=kOutput, calls=%fused_computation.58 | convolution fusion | flops 805404672 | bytes 5439488 | tf_op jit(solution)/shard_map/dot_general | solution.py:161
  172.8 1.1 fusion.68
  173.9 31.2 %all-gather.14.cloned.1.call-done = f32[32,128,128]{2,1,0:T(8,128)} async-done(((f32[4,128,128]{2,1,0:T(8,128)}), f32[32,128,128]{2,1,0:T(8,128)}) %all-gather.14.cloned.1.call-update) | async-done | bytes 2097168 | tf_op jit(solution)/shard_map/all_gather | solution.py:25
  205.1 41.1 %all-gather.18.cloned.1.call-done = f32[32,128,128]{2,1,0:T(8,128)} async-done(((f32[4,128,128]{2,1,0:T(8,128)}), f32[32,128,128]{2,1,0:T(8,128)}) %all-gather.18.cloned.1.call-update) | async-done | bytes 2097168 | tf_op jit(solution)/shard_map/all_gather | solution.py:25
  246.2 1.5 convolution_add_fusion.20
  247.7 1.4 convolution_add_fusion.15
  249.1 1.3 convolution_add_fusion.14
  254.7 7.1 %all-to-all-start = ((bf16[32,2,2,4,128]{4,3,2,1,0:T(4,128)(2,1)}), bf16[32,2,2,4,128]{4,3,2,1,0:T(4,128)(2,1)S(1)}, u32[]{:S(2)}, u32[]{:S(2)}) async-start(bf16[32,2,2,4,128]{4,3,2,1,0:T(4,128)(2,1)} %bitcast.193), calls=%async_computation | async-start | bytes 262144 | tf_op jit(solution)/shard_map/all_to_all | solution.py:42
  261.8 1.6 fusion.38
  265.2 7.1 %all-to-all-done = bf16[32,2,2,4,128]{4,3,2,1,0:T(4,128)(2,1)S(1)} async-done(((bf16[32,2,2,4,128]{4,3,2,1,0:T(4,128)(2,1)}), bf16[32,2,2,4,128]{4,3,2,1,0:T(4,128)(2,1)S(1)}, u32[]{:S(2)}, u32[]{:S(2)}) %all-to-all-start) | async-done | bytes 131104 | tf_op jit(solution)/shard_map/all_to_all | solution.py:42
  272.7 0.7 broadcast_in_dim.80
  273.4 3.8 %all-to-all-start.1 = ((f32[32,1,1024]{2,1,0:T(1,128)}), f32[32,1,1024]{2,1,0:T(1,128)S(1)}, u32[]{:S(2)}, u32[]{:S(2)}) async-start(f32[32,1,1024]{2,1,0:T(1,128)} %broadcast_in_dim.80), calls=%async_computation.1 | async-start | bytes 262144 | tf_op jit(solution)/shard_map/all_to_all | solution.py:48
  277.3 1.7 fusion.60
  279.0 8.8 %all-to-all-done.1 = f32[32,1,1024]{2,1,0:T(1,128)S(1)} async-done(((f32[32,1,1024]{2,1,0:T(1,128)}), f32[32,1,1024]{2,1,0:T(1,128)S(1)}, u32[]{:S(2)}, u32[]{:S(2)}) %all-to-all-start.1) | async-done | bytes 131104 | tf_op jit(solution)/shard_map/all_to_all | solution.py:48
  (155 shorter events, 23.7 us)
Async XLA Ops:
  7.2 39.7 %copy-start = (bf16[4096,256]{1,0:T(8,128)(2,1)S(1)}, bf16[4096,256]{1,0:T(8,128)(2,1)}, u32[]{:S(2)}) copy-start(bf16[4096,256]{1,0:T(8,128)(2,1)} %param.18) | copy-start | bytes 6291460
  7.2 34.8 %all-gather.10.cloned.1.call-start = ((), (), s32[]{:S(2)}) async-start(), calls=%async_computation.2 | async-start | bytes 3538944 | tf_op jit(solution)/shard_map/all_gather | solution.py:185
  7.9 125.4 %all-gather.12.cloned.1.call-start = ((), (), s32[]{:S(2)}) async-start(), calls=%async_computation.3 | async-start | bytes 1310720 | tf_op jit(solution)/shard_map/all_gather | solution.py:25
  49.7 1.6 copy-start.23
  49.7 1.6 copy-start.28
  59.4 3.8 %copy-start.20 = (f32[2,2,3,64,128]{4,3,1,0,2:T(8,128)S(1)}, f32[2,2,3,64,128]{4,3,1,0,2:T(8,128)}, u32[]{:S(2)}) copy-start(f32[2,2,3,64,128]{4,3,1,0,2:T(8,128)} %copy.189) | copy-start | bytes 1179652
  63.3 2.4 copy-start.24
  104.8 0.7 copy-start.4
  104.8 0.8 copy-start.1
  105.6 56.6 %all-gather.16.cloned.1.call-start = ((), (), s32[]{:S(2)}) async-start(), calls=%async_computation.5 | async-start | bytes 1310720 | tf_op jit(solution)/shard_map/all_gather | solution.py:25
  106.3 98.8 %all-gather.14.cloned.1.call-start = ((), (), s32[]{:S(2)}) async-start(), calls=%async_computation.4 | async-start | bytes 2359296 | tf_op jit(solution)/shard_map/all_gather | solution.py:25
  133.3 4.2 %copy-start.3 = (f32[16,128,128]{2,1,0:T(8,128)S(1)}, f32[16,128,128]{2,1,0:T(8,128)}, u32[]{:S(2)}) copy-start(f32[16,128,128]{2,1,0:T(8,128)} %all-gather.12.cloned.1.call-done) | copy-start | bytes 3145732
  134.7 0.7 copy-start.17
  136.8 0.7 copy-start.7
  137.9 0.7 copy-start.9
  139.7 106.4 %all-gather.18.cloned.1.call-start = ((), (), s32[]{:S(2)}) async-start(), calls=%async_computation.6 | async-start | bytes 2359296 | tf_op jit(solution)/shard_map/all_gather | solution.py:25
  162.2 3.5 %copy-start.22 = (f32[16,128,128]{2,1,0:T(8,128)S(1)}, f32[16,128,128]{2,1,0:T(8,128)}, u32[]{:S(2)}) copy-start(f32[16,128,128]{2,1,0:T(8,128)} %all-gather.16.cloned.1.call-done) | copy-start | bytes 3145732
  163.6 4.4 %copy-start.26 = (bf16[2,2,128]{2,1,0:T(2,128)(2,1)S(1)}, bf16[2,2,128]{2,1,0:T(2,128)(2,1)}, u32[]{:S(2)}) copy-start(bf16[2,2,128]{2,1,0:T(2,128)(2,1)} %param.27) | copy-start | bytes 3076
  163.6 4.5 %copy-start.27 = (bf16[2,2,128]{2,1,0:T(2,128)(2,1)S(1)}, bf16[2,2,128]{2,1,0:T(2,128)(2,1)}, u32[]{:S(2)}) copy-start(bf16[2,2,128]{2,1,0:T(2,128)(2,1)} %param.28) | copy-start | bytes 3076
  163.6 4.7 %copy-start.29 = (f32[2,2]{1,0:T(2,128)S(1)}, f32[2,2]{1,0:T(2,128)}, u32[]{:S(2)}) copy-start(f32[2,2]{1,0:T(2,128)} %param.30) | copy-start | bytes 52
  163.6 4.8 %copy-start.32 = (f32[128]{0:T(128)S(1)}, f32[128]{0:T(128)}, u32[]{:S(2)}) copy-start(f32[128]{0:T(128)} %param.26) | copy-start | bytes 1540
  165.0 0.7 copy-start.13
  166.1 0.7 copy-start.15
  168.4 4.3 %copy-start.8 = (f32[4,128,128]{2,1,0:T(8,128)S(1)}, f32[4,128,128]{2,1,0:T(8,128)}, u32[]{:S(2)}) copy-start(f32[4,128,128]{2,1,0:T(8,128)} %copy-done.7) | copy-start | bytes 786436
  168.4 4.3 %copy-start.10 = (f32[4,128,128]{2,1,0:T(8,128)S(1)}, f32[4,128,128]{2,1,0:T(8,128)}, u32[]{:S(2)}) copy-start(f32[4,128,128]{2,1,0:T(8,128)} %copy-done.9) | copy-start | bytes 786436
  168.4 4.3 %copy-start.12 = (f32[4,128,128]{2,1,0:T(8,128)S(1)}, f32[4,128,128]{2,1,0:T(8,128)}, u32[]{:S(2)}) copy-start(f32[4,128,128]{2,1,0:T(8,128)} %fusion.109) | copy-start | bytes 786436
  168.4 4.3 %copy-start.18 = (f32[4,128,128]{2,1,0:T(8,128)S(1)}, f32[4,128,128]{2,1,0:T(8,128)}, u32[]{:S(2)}) copy-start(f32[4,128,128]{2,1,0:T(8,128)} %copy-done.17) | copy-start | bytes 786436
  246.2 3.0 %copy-start.6 = (f32[32,128,128]{2,1,0:T(8,128)S(1)}, f32[32,128,128]{2,1,0:T(8,128)}, u32[]{:S(2)}) copy-start(f32[32,128,128]{2,1,0:T(8,128)} %all-gather.14.cloned.1.call-done) | copy-start | bytes 6291460
  246.2 4.3 %copy-start.19 = (f32[32,128,128]{2,1,0:T(8,128)S(1)}, f32[32,128,128]{2,1,0:T(8,128)}, u32[]{:S(2)}) copy-start(f32[32,128,128]{2,1,0:T(8,128)} %all-gather.18.cloned.1.call-done) | copy-start | bytes 6291460
  251.7 1.0 copy-start.21
  252.1 1.0 copy-start.11
  252.1 1.0 copy-start.14
  252.1 1.1 copy-start.16
  252.1 1.5 copy-start.2
  252.1 1.5 copy-start.5
  254.7 17.6 %all-to-all-start = ((bf16[32,2,2,4,128]{4,3,2,1,0:T(4,128)(2,1)}), bf16[32,2,2,4,128]{4,3,2,1,0:T(4,128)(2,1)S(1)}, u32[]{:S(2)}, u32[]{:S(2)}) async-start(bf16[32,2,2,4,128]{4,3,2,1,0:T(4,128)(2,1)} %bitcast.193), calls=%async_computation | async-start | bytes 262144 | tf_op jit(solution)/shard_map/all_to_all | solution.py:42
  263.9 24.0 %copy-start.30 = (bf16[2,2,128]{2,1,0:T(2,128)(2,1)S(1)}, bf16[2,2,128]{2,1,0:T(2,128)(2,1)}, u32[]{:S(2)}) copy-start(bf16[2,2,128]{2,1,0:T(2,128)(2,1)} %param.29) | copy-start | bytes 3076
  263.9 24.0 %copy-start.31 = (f32[2,2]{1,0:T(2,128)S(1)}, f32[2,2]{1,0:T(2,128)}, u32[]{:S(2)}) copy-start(f32[2,2]{1,0:T(2,128)} %param.31) | copy-start | bytes 52
  272.4 16.4 %copy-start.25 = (bf16[2,2,4,128]{3,2,1,0:T(4,128)(2,1)}, bf16[2,2,4,128]{3,2,1,0:T(4,128)(2,1)S(1)}, u32[]{:S(2)}) copy-start(bf16[2,2,4,128]{3,2,1,0:T(4,128)(2,1)S(1)} %reduce_sum.87) | copy-start | bytes 12292
  273.4 14.4 %all-to-all-start.1 = ((f32[32,1,1024]{2,1,0:T(1,128)}), f32[32,1,1024]{2,1,0:T(1,128)S(1)}, u32[]{:S(2)}, u32[]{:S(2)}) async-start(f32[32,1,1024]{2,1,0:T(1,128)} %broadcast_in_dim.80), calls=%async_computation.1 | async-start | bytes 262144 | tf_op jit(solution)/shard_map/all_to_all | solution.py:48
Sparse Core Ops, SparseCore 0:
  9.8 32.1 all-gather.9
  105.7 27.5 all-gather.11
  135.1 27.0 all-gather.15
  163.8 41.2 all-gather.13
  206.7 39.4 all-gather.17
where the time goes:
time: 296 us; the launch traced here: 295 us
  waiting for transfers between devices  172 us (58%)
  matrix products  75.5 us (26%)
  between operations  14.6 us (5%)
  local copies, waits for them, and re-layouts  13.8 us (5%)
  starting transfers between devices  11.1 us (4%)
  other arithmetic  8.51 us (3%)
    all_gather x4, waiting for transfers between devices, carried_in(): pieces = jax.tree.map(lambda part: lax.all_gather(part, axis), subtotal)  122 us
    dot_general x61, matrix products, matmul(): return jnp.einsum(form, left, right, precision=highest)  55.6 us
    all_gather x1, waiting for transfers between devices, shards(): lax.all_gather(tokens, 'tp', axis=2, tiled=True)  32.6 us
    dot_general x6, matrix products, project_rows(): jnp.dot(flat_rows, weight, preferred_element_type=jnp.float32)  19.9 us
    all_to_all x1, waiting for transfers between devices, copy_for_each(): lax.all_to_all(jnp.broadcast_to(value[None], (length, *value.shape)), axi...  8.81 us
    all_to_all x1, waiting for transfers between devices, summed_on_arrival(): lax.all_to_all(parts, axis, split_axis=0, concat_axis=0, tiled=True)  7.1 us
    all_to_all x1, starting transfers between devices, summed_on_arrival(): lax.all_to_all(parts, axis, split_axis=0, concat_axis=0, tiled=True)  7.08 us
  transfers between devices with their start and end apart: 7, of which 7 were waited for; matrix products, arithmetic and copies ran while one was open for 7% of the time, Pallas kernels for 0%

commit v1 on v0

--- a/solution.py
+++ b/solution.py
@@ -1,3 +1,4 @@
+import functools
 import jax
 import jax.numpy as jnp
 from jax import lax
@@ -9,6 +10,15 @@
 unit_floor = 1.0
 norm_floor = 0.001
 highest = lax.Precision.HIGHEST
+
+
+def _supply_all_object(raw, row_axis, dim_i):
+    latest = jnp.stack([raw for _ in range(jax.lax.axis_size(row_axis))], axis=0)
+    current_block = jax.lax.all_to_all(latest, row_axis, 0, 0)
+    return jnp.concatenate(current_block, axis=dim_i)
+
+
+finish_lines = functools.partial(_supply_all_object, row_axis="tp", dim_i=2)
 
 
 def neutral_like(value, identity):
@@ -182,7 +192,7 @@
     seq_count, span_len, _ = tokens.shape
     head_count = rate_log.shape[0]
     weights = (query_weight, key_weight, value_weight, gate_weight, beta_weight, decay_weight)
-    totals = project_rows(lax.all_gather(tokens, "tp", axis=2, tiled=True), weights)
+    totals = project_rows(finish_lines(tokens), weights)
     query_rows = stored(totals[0])
     key_rows = stored(totals[1])
     value_rows = stored(totals[2])

time: 296 us -> 314 us (1.061)
  local copies, waits for them, and re-layouts: 13.8 us -> 23.1 us
  starting transfers between devices: 11.1 us -> 17.8 us
    all_to_all x0 -> x1, waiting for transfers between devices: none -> 36.3 us  [_supply_all_object(): current_block = jax.lax.all_to_all(latest, row_axis, 0, 0)]
    all_gather x1 -> x0, waiting for transfers between devices: 32.6 us -> none  [shards(): lax.all_gather(tokens, 'tp', axis=2, tiled=True)]
    all_to_all x0 -> x1, starting transfers between devices: none -> 6.63 us  [_supply_all_object(): current_block = jax.lax.all_to_all(latest, row_axis, 0, 0)]
    reshape x0 -> x1, local copies, waits for them, and re-layouts: none -> 3.64 us  [_supply_all_object(): return jnp.concatenate(current_block, axis=dim_i)]
    unnamed x68 -> x81, local copies, waits for them, and re-layouts: 5.89 us -> 8.38 us
  transfers between devices with their start and end apart: 7 -> 7, of which waited for: 7 -> 7; matrix products, arithmetic and copies ran while one was open for 7% -> 6% of each run, Pallas kernels for 0% -> 0%
where the time goes in v1:
time: 314 us; the launch traced here: 313 us
  waiting for transfers between devices  174 us (55%)
  matrix products  73.8 us (24%)
  local copies, waits for them, and re-layouts  23.1 us (7%)
  starting transfers between devices  17.8 us (6%)
  between operations  14.6 us (5%)
  other arithmetic  8.87 us (3%)
    all_gather x4, waiting for transfers between devices, carried_in(): pieces = jax.tree.map(lambda part: lax.all_gather(part, axis), subtotal)  122 us
    dot_general x61, matrix products, matmul(): return jnp.einsum(form, left, right, precision=highest)  55.8 us
    all_to_all x1, waiting for transfers between devices, _supply_all_object(): current_block = jax.lax.all_to_all(latest, row_axis, 0, 0)  36.3 us
    dot_general x6, matrix products, project_rows(): jnp.dot(flat_rows, weight, preferred_element_type=jnp.float32)  18 us
    all_to_all x1, waiting for transfers between devices, copy_for_each(): lax.all_to_all(jnp.broadcast_to(value[None], (length, *value.shape)), axi...  8.81 us
    unnamed x81, local copies, waits for them, and re-layouts  8.38 us
    all_to_all x1, starting transfers between devices, summed_on_arrival(): lax.all_to_all(parts, axis, split_axis=0, concat_axis=0, tiled=True)  7.2 us
    all_to_all x1, waiting for transfers between devices, summed_on_arrival(): lax.all_to_all(parts, axis, split_axis=0, concat_axis=0, tiled=True)  7.07 us
  transfers between devices with their start and end apart: 7, of which 7 were waited for; matrix products, arithmetic and copies ran while one was open for 6% of the time, Pallas kernels for 0%

profile of v1, /device:TPU:8, one launch (start us, length us, event | category | flops | bytes accessed | tf_op | source)
XLA Modules:
  0.0 313.0 jit_solution(3897987379828684881)
XLA Ops:
  7.2 3.1 %stack.2 = bf16[8,2,192,512]{3,2,1,0:T(8,128)(2,1)} broadcast(bf16[2,192,512]{2,1,0:T(8,128)(2,1)} %param.17), dimensions={1,2,3} | broadcast | bytes 3538944 | tf_op jit(solution)/shard_map/stack | solution.py:16
  10.3 6.6 %all-to-all-start = ((bf16[8,2,192,512]{3,2,1,0:T(8,128)(2,1)}), bf16[8,2,192,512]{3,2,1,0:T(8,128)(2,1)}, u32[]{:S(2)}, u32[]{:S(2)}) async-start(bf16[8,2,192,512]{3,2,1,0:T(8,128)(2,1)} %stack.2), calls=%async_computation | async-start | bytes 6291456 | tf_op jit(solution)/shard_map/all_to_all | solution.py:17
  17.7 36.3 %all-to-all-done = bf16[8,2,192,512]{3,2,1,0:T(8,128)(2,1)} async-done(((bf16[8,2,192,512]{3,2,1,0:T(8,128)(2,1)}), bf16[8,2,192,512]{3,2,1,0:T(8,128)(2,1)}, u32[]{:S(2)}, u32[]{:S(2)}) %all-to-all-start) | async-done | bytes 3145760 | tf_op jit(solution)/shard_map/all_to_all | solution.py:17
  54.0 3.6 %copy.180 = bf16[2,192,8,512]{3,2,1,0:T(8,128)(2,1)S(1)} copy(bf16[2,192,8,512]{3,1,0,2:T(8,128)(2,1)} %bitcast) | data formatting | bytes 6291456 | tf_op jit(solution)/shard_map/reshape | solution.py:18
  57.7 1.4 copy.234
  59.1 1.6 copy-done.3
  60.7 0.9 fusion.91
  61.8 1.1 reduce_window_sum.11
  63.8 2.9 convolution_convert_fusion.1
  67.4 0.8 copy.194
  68.3 2.8 fusion.50
  71.2 3.5 %convolution_convert_fusion.3 = bf16[384,256]{1,0:T(8,128)(2,1)S(1)} fusion(bf16[384,4096]{1,0:T(8,128)(2,1)} %bitcast.239, bf16[4096,256]{1,0:T(8,128)(2,1)} %param.19), kind=kOutput, calls=%fused_computation.61 | convolution fusion | flops 805404672 | bytes 5439488 | tf_op jit(solution)/shard_map/dot_general | solution.py:171
  75.5 0.8 copy.183
  76.4 3.6 %convolution_convert_fusion.2 = bf16[384,256]{1,0:T(8,128)(2,1)S(1)} fusion(bf16[384,4096]{1,0:T(8,128)(2,1)} %bitcast.240, bf16[4096,256]{1,0:T(8,128)(2,1)} %param.20), kind=kOutput, calls=%fused_computation.60 | convolution fusion | flops 805404672 | bytes 5439488 | tf_op jit(solution)/shard_map/dot_general | solution.py:171
  80.2 1.5 multiply_bitcast_fusion
  81.7 0.9 multiply_bitcast_fusion.1
  82.6 0.8 fusion.41
  88.7 1.3 convolution_bitcast_fusion.4
  90.0 0.7 convolution_bitcast_fusion.3
  90.7 1.5 fusion.39
  92.3 29.6 %while.17 = (s32[]{:T(128)}, f32[4,128,128]{2,1,0:T(8,128)S(1)}, f32[4,128,128]{2,1,0:T(8,128)S(1)}, f32[3,4,64,128]{3,2,0,1:T(8,128)}, f32[3,4,64,128]{3,2,0,1:...) while((s32[]{:T(128)}, f32[4,128,128]{2,1,0:T(8,128)S(1)}, ...), condition=%wide.region_4.5_spmd.clone, body=%wide.region_3.4_spmd.clone.sunk | while | flops 403210240 | bytes 5445847 | solution.py:233
  92.3 1.3 convolution_subtract_fusion.6
  93.6 1.2 fusion.226
  94.8 1.0 fusion.227
  96.5 1.5 convolution_add_fusion.23
  98.0 1.2 convolution_subtract_fusion.8
  99.2 1.0 fusion.228
  100.3 1.5 convolution_subtract_fusion.7
  102.2 1.3 convolution_subtract_fusion.6
  103.5 1.2 fusion.226
  104.6 1.0 fusion.227
  106.3 1.5 convolution_add_fusion.23
  107.9 1.2 convolution_subtract_fusion.8
  109.1 1.1 fusion.228
  110.1 1.5 convolution_subtract_fusion.7
  112.0 1.3 convolution_subtract_fusion.6
  113.3 1.2 fusion.226
  114.5 1.0 fusion.227
  116.2 1.5 convolution_add_fusion.23
  117.7 1.2 convolution_subtract_fusion.8
  118.9 1.0 fusion.228
  120.0 1.5 convolution_subtract_fusion.7
  123.4 26.2 %all-gather.9.cloned.1.call-done = f32[16,128,128]{2,1,0:T(8,128)} async-done(((f32[4,128,128]{2,1,0:T(8,128)}), f32[16,128,128]{2,1,0:T(8,128)}) %all-gather.9.cloned.1.call-update) | async-done | bytes 1048592 | tf_op jit(solution)/shard_map/all_gather | solution.py:35
  149.7 1.4 fusion.76
  151.8 1.3 fusion.107
  154.3 1.1 fusion.109
  155.5 23.0 %all-gather.13.cloned.1.call-done = f32[16,128,128]{2,1,0:T(8,128)} async-done(((f32[4,128,128]{2,1,0:T(8,128)}), f32[16,128,128]{2,1,0:T(8,128)}) %all-gather.13.cloned.1.call-update) | async-done | bytes 1048592 | tf_op jit(solution)/shard_map/all_gather | solution.py:35
  178.5 1.4 convolution_add_fusion.19
  180.0 1.5 convolution_add_fusion.18
  183.3 1.1 convolution_add_fusion.16
  185.0 4.3 %convolution_convert_fusion = bf16[384,256]{1,0:T(8,128)(2,1)} fusion(bf16[384,4096]{1,0:T(8,128)(2,1)} %bitcast.241, bf16[4096,256]{1,0:T(8,128)(2,1)} %param.21), kind=kOutput, calls=%fused_computation.58 | convolution fusion | flops 805404672 | bytes 5439488 | tf_op jit(solution)/shard_map/dot_general | solution.py:171
  189.3 1.1 fusion.68
  190.4 31.2 %all-gather.11.cloned.1.call-done = f32[32,128,128]{2,1,0:T(8,128)} async-done(((f32[4,128,128]{2,1,0:T(8,128)}), f32[32,128,128]{2,1,0:T(8,128)}) %all-gather.11.cloned.1.call-update) | async-done | bytes 2097168 | tf_op jit(solution)/shard_map/all_gather | solution.py:35
  221.6 41.1 %all-gather.15.cloned.1.call-done = f32[32,128,128]{2,1,0:T(8,128)} async-done(((f32[4,128,128]{2,1,0:T(8,128)}), f32[32,128,128]{2,1,0:T(8,128)}) %all-gather.15.cloned.1.call-update) | async-done | bytes 2097168 | tf_op jit(solution)/shard_map/all_gather | solution.py:35
  262.7 1.5 convolution_add_fusion.20
  264.2 1.4 convolution_add_fusion.15
  265.7 1.3 convolution_add_fusion.14
  271.4 7.2 %all-to-all-start.1 = ((bf16[32,2,2,4,128]{4,3,2,1,0:T(4,128)(2,1)}), bf16[32,2,2,4,128]{4,3,2,1,0:T(4,128)(2,1)}, u32[]{:S(2)}, u32[]{:S(2)}) async-start(bf16[32,2,2,4,128]{4,3,2,1,0:T(4,128)(2,1)} %bitcast.196), calls=%async_computation.1 | async-start | bytes 262144 | tf_op jit(solution)/shard_map/all_to_all | solution.py:52
  278.6 1.6 fusion.38
  282.0 7.1 %all-to-all-done.1 = bf16[32,2,2,4,128]{4,3,2,1,0:T(4,128)(2,1)} async-done(((bf16[32,2,2,4,128]{4,3,2,1,0:T(4,128)(2,1)}), bf16[32,2,2,4,128]{4,3,2,1,0:T(4,128)(2,1)}, u32[]{:S(2)}, u32[]{:S(2)}) %all-to-all-start.1) | async-done | bytes 131104 | tf_op jit(solution)/shard_map/all_to_all | solution.py:52
  289.0 1.0 reduce_sum.87
  291.0 3.8 %all-to-all-start.2 = ((f32[32,1,1024]{2,1,0:T(1,128)}), f32[32,1,1024]{2,1,0:T(1,128)S(1)}, u32[]{:S(2)}, u32[]{:S(2)}) async-start(f32[32,1,1024]{2,1,0:T(1,128)} %broadcast_in_dim.80), calls=%async_computation.2 | async-start | bytes 262144 | tf_op jit(solution)/shard_map/all_to_all | solution.py:58
  294.9 1.7 fusion.60
  296.6 8.8 %all-to-all-done.2 = f32[32,1,1024]{2,1,0:T(1,128)S(1)} async-done(((f32[32,1,1024]{2,1,0:T(1,128)}), f32[32,1,1024]{2,1,0:T(1,128)S(1)}, u32[]{:S(2)}, u32[]{:S(2)}) %all-to-all-start.2) | async-done | bytes 131104 | tf_op jit(solution)/shard_map/all_to_all | solution.py:58
  (169 shorter events, 25.8 us)
Async XLA Ops:
  7.2 56.6 %copy-start = (bf16[4096,256]{1,0:T(8,128)(2,1)S(1)}, bf16[4096,256]{1,0:T(8,128)(2,1)}, u32[]{:S(2)}) copy-start(bf16[4096,256]{1,0:T(8,128)(2,1)} %param.18) | copy-start | bytes 6291460
  10.3 6.7 %copy-start.38 = (f32[2]{0:T(128)S(1)}, f32[2]{0:T(128)}, u32[]{:S(2)}) copy-start(f32[2]{0:T(128)} %param.25) | copy-start | bytes 28
  10.3 43.7 %all-to-all-start = ((bf16[8,2,192,512]{3,2,1,0:T(8,128)(2,1)}), bf16[8,2,192,512]{3,2,1,0:T(8,128)(2,1)}, u32[]{:S(2)}, u32[]{:S(2)}) async-start(bf16[8,2,192,512]{3,2,1,0:T(8,128)(2,1)} %stack.2), calls=%async_computation | async-start | bytes 6291456 | tf_op jit(solution)/shard_map/all_to_all | solution.py:17
  16.9 132.7 %all-gather.9.cloned.1.call-start = ((), (), s32[]{:S(2)}) async-start(), calls=%async_computation.3 | async-start | bytes 1310720 | tf_op jit(solution)/shard_map/all_gather | solution.py:35
  57.7 3.1 copy-start.26
  59.1 1.6 copy-start.3
  66.7 1.6 copy-start.27
  66.7 1.6 copy-start.32
  76.4 3.8 %copy-start.23 = (f32[2,2,3,64,128]{4,3,1,0,2:T(8,128)S(1)}, f32[2,2,3,64,128]{4,3,1,0,2:T(8,128)}, u32[]{:S(2)}) copy-start(f32[2,2,3,64,128]{4,3,1,0,2:T(8,128)} %copy.194) | copy-start | bytes 1179652
  80.2 2.4 copy-start.28
  121.9 0.7 copy-start.5
  121.9 0.8 copy-start.1
  122.6 55.9 %all-gather.13.cloned.1.call-start = ((), (), s32[]{:S(2)}) async-start(), calls=%async_computation.5 | async-start | bytes 1310720 | tf_op jit(solution)/shard_map/all_gather | solution.py:35
  123.4 98.2 %all-gather.11.cloned.1.call-start = ((), (), s32[]{:S(2)}) async-start(), calls=%async_computation.4 | async-start | bytes 2359296 | tf_op jit(solution)/shard_map/all_gather | solution.py:35
  149.7 3.5 %copy-start.4 = (f32[16,128,128]{2,1,0:T(8,128)S(1)}, f32[16,128,128]{2,1,0:T(8,128)}, u32[]{:S(2)}) copy-start(f32[16,128,128]{2,1,0:T(8,128)} %all-gather.9.cloned.1.call-done) | copy-start | bytes 3145732
  151.1 0.7 copy-start.20
  153.1 2.3 copy-start.10
  153.6 0.7 copy-start.12
  155.4 107.3 %all-gather.15.cloned.1.call-start = ((), (), s32[]{:S(2)}) async-start(), calls=%async_computation.6 | async-start | bytes 2359296 | tf_op jit(solution)/shard_map/all_gather | solution.py:35
  178.5 3.6 %copy-start.25 = (f32[16,128,128]{2,1,0:T(8,128)S(1)}, f32[16,128,128]{2,1,0:T(8,128)}, u32[]{:S(2)}) copy-start(f32[16,128,128]{2,1,0:T(8,128)} %all-gather.13.cloned.1.call-done) | copy-start | bytes 3145732
  179.9 4.5 %copy-start.8 = (f32[4,128,128]{2,1,0:T(8,128)}, f32[4,128,128]{2,1,0:T(8,128)S(1)}, u32[]{:S(2)}) copy-start(f32[4,128,128]{2,1,0:T(8,128)S(1)} %convolution_add_fusion.19) | copy-start | bytes 786436
  179.9 4.5 %copy-start.30 = (bf16[2,2,128]{2,1,0:T(2,128)(2,1)S(1)}, bf16[2,2,128]{2,1,0:T(2,128)(2,1)}, u32[]{:S(2)}) copy-start(bf16[2,2,128]{2,1,0:T(2,128)(2,1)} %param.27) | copy-start | bytes 3076
  180.0 4.6 %copy-start.31 = (bf16[2,2,128]{2,1,0:T(2,128)(2,1)S(1)}, bf16[2,2,128]{2,1,0:T(2,128)(2,1)}, u32[]{:S(2)}) copy-start(bf16[2,2,128]{2,1,0:T(2,128)(2,1)} %param.28) | copy-start | bytes 3076
  180.0 4.9 %copy-start.33 = (f32[2,2]{1,0:T(2,128)S(1)}, f32[2,2]{1,0:T(2,128)}, u32[]{:S(2)}) copy-start(f32[2,2]{1,0:T(2,128)} %param.30) | copy-start | bytes 52
  180.0 5.0 %copy-start.36 = (f32[128]{0:T(128)S(1)}, f32[128]{0:T(128)}, u32[]{:S(2)}) copy-start(f32[128]{0:T(128)} %param.26) | copy-start | bytes 1540
  181.4 0.7 copy-start.16
  182.6 0.7 copy-start.18
  184.9 4.3 %copy-start.11 = (f32[4,128,128]{2,1,0:T(8,128)S(1)}, f32[4,128,128]{2,1,0:T(8,128)}, u32[]{:S(2)}) copy-start(f32[4,128,128]{2,1,0:T(8,128)} %copy-done.10) | copy-start | bytes 786436
  184.9 4.3 %copy-start.13 = (f32[4,128,128]{2,1,0:T(8,128)S(1)}, f32[4,128,128]{2,1,0:T(8,128)}, u32[]{:S(2)}) copy-start(f32[4,128,128]{2,1,0:T(8,128)} %copy-done.12) | copy-start | bytes 786436
  184.9 4.3 %copy-start.15 = (f32[4,128,128]{2,1,0:T(8,128)S(1)}, f32[4,128,128]{2,1,0:T(8,128)}, u32[]{:S(2)}) copy-start(f32[4,128,128]{2,1,0:T(8,128)} %fusion.109) | copy-start | bytes 786436
  185.0 4.3 %copy-start.21 = (f32[4,128,128]{2,1,0:T(8,128)S(1)}, f32[4,128,128]{2,1,0:T(8,128)}, u32[]{:S(2)}) copy-start(f32[4,128,128]{2,1,0:T(8,128)} %copy-done.20) | copy-start | bytes 786436
  262.7 3.0 copy-start.7
  262.7 4.3 %copy-start.22 = (f32[32,128,128]{2,1,0:T(8,128)S(1)}, f32[32,128,128]{2,1,0:T(8,128)}, u32[]{:S(2)}) copy-start(f32[32,128,128]{2,1,0:T(8,128)} %all-gather.15.cloned.1.call-done) | copy-start | bytes 6291460
  268.2 1.0 copy-start.24
  268.6 1.0 copy-start.9
  268.6 1.0 copy-start.14
  268.7 1.1 copy-start.17
  268.7 1.2 copy-start.19
  268.7 1.6 copy-start.2
  268.7 1.6 copy-start.6
  271.4 17.7 %all-to-all-start.1 = ((bf16[32,2,2,4,128]{4,3,2,1,0:T(4,128)(2,1)}), bf16[32,2,2,4,128]{4,3,2,1,0:T(4,128)(2,1)}, u32[]{:S(2)}, u32[]{:S(2)}) async-start(bf16[32,2,2,4,128]{4,3,2,1,0:T(4,128)(2,1)} %bitcast.196), calls=%async_computation.1 | async-start | bytes 262144 | tf_op jit(solution)/shard_map/all_to_all | solution.py:52
  280.7 24.9 %copy-start.34 = (bf16[2,2,128]{2,1,0:T(2,128)(2,1)S(1)}, bf16[2,2,128]{2,1,0:T(2,128)(2,1)}, u32[]{:S(2)}) copy-start(bf16[2,2,128]{2,1,0:T(2,128)(2,1)} %param.29) | copy-start | bytes 3076
  280.7 24.9 %copy-start.35 = (f32[2,2]{1,0:T(2,128)S(1)}, f32[2,2]{1,0:T(2,128)}, u32[]{:S(2)}) copy-start(f32[2,2]{1,0:T(2,128)} %param.31) | copy-start | bytes 52
  280.7 25.1 %copy-start.37 = (f32[128]{0:T(128)S(1)}, f32[128]{0:T(128)}, u32[]{:S(2)}) copy-start(f32[128]{0:T(128)} %param.26) | copy-start | bytes 1540
  290.0 16.4 %copy-start.29 = (bf16[2,2,4,128]{3,2,1,0:T(4,128)(2,1)}, bf16[2,2,4,128]{3,2,1,0:T(4,128)(2,1)S(1)}, u32[]{:S(2)}) copy-start(bf16[2,2,4,128]{3,2,1,0:T(4,128)(2,1)S(1)} %reduce_sum.87) | copy-start | bytes 12292
  291.0 14.4 %all-to-all-start.2 = ((f32[32,1,1024]{2,1,0:T(1,128)}), f32[32,1,1024]{2,1,0:T(1,128)S(1)}, u32[]{:S(2)}, u32[]{:S(2)}) async-start(f32[32,1,1024]{2,1,0:T(1,128)} %broadcast_in_dim.80), calls=%async_computation.2 | async-start | bytes 262144 | tf_op jit(solution)/shard_map/all_to_all | solution.py:58
Sparse Core Ops, SparseCore 0:
  122.8 26.8 all-gather.8
  151.5 27.0 all-gather.12
  180.3 41.2 all-gather.10
  223.2 39.4 all-gather.14
